TPU v7x, 32 devices: a whole 2x2x4 slice. The times are simulated.
32 devices in a mesh: sp: 8 (over z, y), tp: 4 (over x, core).
Axes of the slice: x: 2, y: 2, z: 4, core: 2. Of those that a mesh axis runs over, the one named last changes fastest.
Arguments:
- residual_entry_input: bfloat16 [8192, 2048], P(('sp', 'tp')), may hold values from -6 to 6
- query_matrix_rows: bfloat16 [8192, 1024], P('sp', 'tp'), may hold values from -6 to 6
- key_matrix_rows: bfloat16 [8192, 1024], P('sp', 'tp'), may hold values from -6 to 6
- value_matrix_rows: bfloat16 [8192, 2048], P('sp', 'tp'), may hold values from -6 to 6
- output_gate_logits: bfloat16 [8192, 2048], P('sp', 'tp'), may hold values from -6 to 6
- input_gate_logits: float32 [8192, 8], P('sp', 'tp'), may hold values from -6 to 6
- forget_gate_logits: float32 [8192, 8], P('sp', 'tp'), may hold values from -8 to 31
- forget_decay_offset: float32 [8192, 8], P('sp', 'tp'), may hold values from -0.7 to 0
- head_norm_gain: float32 [8, 256], P('tp'), may hold values from 0.1 to 1.9
- cell_output_weight: bfloat16 [2048, 2048], P('tp'), may hold values from -0.125 to 0.125
- feedforward_norm_gain: float32 [2048], replicated, may hold values from 0.1 to 1.9
- gate_up_weight: bfloat16 [2048, 5632], P('sp', 'tp'), may hold values from -0.125 to 0.125
- value_up_weight: bfloat16 [2048, 5632], P('sp', 'tp'), may hold values from -0.125 to 0.125
- gate_filter_taps: float32 [3, 5632], P(None, 'tp'), may hold values from -3 to 3
- value_filter_taps: float32 [3, 5632], P(None, 'tp'), may hold values from -3 to 3
- down_projection_weight: bfloat16 [5632, 2048], P('tp', 'sp'), may hold values from -0.078125 to 0.078125
Outputs:
- result: bfloat16 [8192, 2048], P(('sp', 'tp'))
All inputs are finite; a program needn't handle non-finite values.
Results may differ from a plain program's by a relative error of at most 0.025.
Values may be sent and summed in bfloat16 or wider, within the bound.
No kernel may reach another device: no remote copies, remote signals or barrier semaphores. Data moves between devices by JAX's collectives and lax.ppermute only.
A program may use at most 128 MiB of HBM per device.

v0:
```python
import jax
import jax.numpy as jnp
from jax import lax
from jax.sharding import PartitionSpec as P

BLOCK = 128
eps = 1e-06
neg_large = -1e30


def carried_in(x, axis, combine, identity):
    count, position = (lax.axis_size(axis), lax.axis_index(axis))
    everything = jax.tree.map(
        lambda part, kind: lax.all_gather(part.astype(kind), axis),
        x,
        (jnp.bfloat16, jnp.bfloat16, jnp.bfloat16, jnp.bfloat16),
    )
    start = jax.tree.map(
        lambda part, zero: jnp.broadcast_to(jnp.asarray(zero, part.dtype), part.shape), x, identity
    )

    def lap(k, before):
        reached = k < position
        new = combine(
            before, jax.tree.map(lambda part, own: part[k].astype(own.dtype), everything, x)
        )
        return jax.tree.map(lambda a, b: jnp.where(reached, a, b), new, before)

    return lax.fori_loop(0, count, lap, start)


def shifted(x, axis, by):
    count = lax.axis_size(axis)
    pairs = [(i, i + by) for i in range(count) if 0 <= i + by < count]
    return lax.ppermute(x, axis, pairs)


def gate_log_values(input_gate_logits, forget_gate_logits, forget_decay_offset):
    input_log_value = 15.0 * jnp.tanh(input_gate_logits / 15.0)
    forget_log_sigmoid = (
        jax.nn.log_sigmoid(15.0 * jnp.tanh(forget_gate_logits / 15.0)) + forget_decay_offset
    )
    return (input_log_value, forget_log_sigmoid)


def combine_states(earlier, later):
    total_one, memory_one, normer_one, running_one = earlier
    total_two, memory_two, normer_two, running_two = later
    joined = jnp.maximum(total_two + running_one, running_two)
    weight_one = jnp.exp(total_two + running_one - joined)
    weight_two = jnp.exp(running_two - joined)
    memory = weight_one[:, None, None] * memory_one + weight_two[:, None, None] * memory_two
    normer = weight_one[:, None] * normer_one + weight_two[:, None] * normer_two
    return (total_one + total_two, memory, normer, joined)


def local_step(state_carry, inputs):
    memory, normer, running = state_carry
    query_block, key_block, value_block, input_block, forget_block = inputs
    length = query_block.shape[0]
    highest = lax.Precision.HIGHEST
    query_scale = query_block.shape[2] ** (-0.5)
    causal = jnp.tril(jnp.ones((length, length), dtype=bool))[:, :, None]
    cumulative = jnp.cumsum(forget_block, axis=0)
    logits = cumulative[:, None, :] - cumulative[None, :, :] + input_block[None, :, :]
    logits = jnp.where(causal, logits, -jnp.inf)
    carried = cumulative + running[None, :]
    stable = jnp.maximum(carried, jnp.max(logits, axis=1))
    carry_weight = jnp.exp(carried - stable)
    raw = (
        jnp.einsum("thd,shd->tsh", query_block, key_block, preferred_element_type=jnp.float32)
        * query_scale
    )
    scores = raw * jnp.exp(logits - stable[:, None, :])
    scaled_query = query_block.astype(jnp.float32) * query_scale
    numerator = carry_weight[:, :, None] * jnp.einsum(
        "hvd,thd->thv", memory, scaled_query, precision=highest
    )
    numerator = numerator + jnp.einsum(
        "tsh,shv->thv", scores.astype(jnp.bfloat16), value_block, preferred_element_type=jnp.float32
    )
    denominator = carry_weight * jnp.einsum(
        "hd,thd->th", normer, scaled_query, precision=highest
    ) + jnp.sum(scores, axis=1)
    last_sum = cumulative[-1]
    weights_log = last_sum[None, :] - cumulative + input_block
    new_running = jnp.maximum(last_sum + running, jnp.max(weights_log, axis=0))
    decay_factor = jnp.exp(last_sum + running - new_running)
    weighted = (
        key_block.astype(jnp.float32) * jnp.exp(weights_log - new_running[None, :])[:, :, None]
    )
    memory = decay_factor[:, None, None] * memory + jnp.einsum(
        "shv,shd->hvd",
        value_block,
        weighted.astype(jnp.bfloat16),
        preferred_element_type=jnp.float32,
    )
    normer = decay_factor[:, None] * normer + jnp.sum(weighted, axis=0)
    return ((memory, normer, new_running), (numerator, denominator, stable))


def local(
    residual_entry_input,
    query_matrix_rows,
    key_matrix_rows,
    value_matrix_rows,
    output_gate_logits,
    input_gate_logits,
    forget_gate_logits,
    forget_decay_offset,
    head_norm_gain,
    cell_output_weight,
    feedforward_norm_gain,
    gate_up_weight,
    value_up_weight,
    gate_filter_taps,
    value_filter_taps,
    down_projection_weight,
):
    highest = lax.Precision.HIGHEST
    token_count = query_matrix_rows.shape[0]
    head_count = input_gate_logits.shape[1]
    key_width = query_matrix_rows.shape[1] // head_count
    value_width = value_matrix_rows.shape[1] // head_count
    query_scale = key_width ** (-0.5)
    queries_low = query_matrix_rows.reshape(token_count, head_count, key_width)
    keys_low = key_matrix_rows.reshape(token_count, head_count, key_width)
    values_low = value_matrix_rows.reshape(token_count, head_count, value_width)
    input_log_value, forget_log_sigmoid = gate_log_values(
        input_gate_logits, forget_gate_logits, forget_decay_offset
    )
    cumulative = jnp.cumsum(forget_log_sigmoid, axis=0)
    total_log = cumulative[-1]
    block_count = token_count // BLOCK

    def blocks(tensor):
        return tensor.reshape((block_count, BLOCK) + tensor.shape[1:])

    initial = (
        jnp.zeros((head_count, value_width, key_width), jnp.float32),
        jnp.zeros((head_count, key_width), jnp.float32),
        jnp.full((head_count,), neg_large, jnp.float32),
    )
    end_state, (numerator, denominator, stable) = lax.scan(
        local_step,
        initial,
        (
            blocks(queries_low),
            blocks(keys_low),
            blocks(values_low),
            blocks(input_log_value),
            blocks(forget_log_sigmoid),
        ),
    )
    end_memory, end_normer, end_running = end_state
    identity = (
        jnp.zeros((head_count,), jnp.float32),
        jnp.zeros((head_count, value_width, key_width), jnp.float32),
        jnp.zeros((head_count, key_width), jnp.float32),
        jnp.full((head_count,), neg_large, jnp.float32),
    )
    prefix = carried_in(
        (total_log, end_memory, end_normer, end_running), "sp", combine_states, identity
    )
    numerator = numerator.reshape(token_count, head_count, value_width)
    denominator = denominator.reshape(token_count, head_count)
    stable = stable.reshape(token_count, head_count)
    _, prior_memory, prior_normer, prior_running = prefix
    scaled_query = queries_low.astype(jnp.float32) * query_scale
    prior_log = cumulative + prior_running[None, :]
    top_log = jnp.maximum(stable, prior_log)
    local_weight = jnp.exp(stable - top_log)
    prior_weight = jnp.exp(prior_log - top_log)
    numerator = local_weight[:, :, None] * numerator + prior_weight[:, :, None] * jnp.einsum(
        "hvd,thd->thv", prior_memory, scaled_query, precision=highest
    )
    denominator = local_weight * denominator + prior_weight * jnp.einsum(
        "hd,thd->th", prior_normer, scaled_query, precision=highest
    )
    memory_out = numerator / jnp.maximum(jnp.abs(denominator), jnp.exp(-top_log))[:, :, None]
    normed = (
        memory_out
        * lax.rsqrt(jnp.mean(memory_out * memory_out, axis=-1, keepdims=True) + eps)
        * head_norm_gain[None, :, :]
    )
    gated_rows = (
        normed.reshape(token_count, head_count * value_width)
        * jax.nn.sigmoid(output_gate_logits.astype(jnp.float32))
    ).astype(jnp.bfloat16)
    whole_out = lax.all_gather(cell_output_weight, "tp", axis=0, tiled=True)
    own_rows = lax.all_to_all(gated_rows, "tp", split_axis=0, concat_axis=1, tiled=True)
    mixed_rows = jnp.dot(own_rows, whole_out, preferred_element_type=jnp.float32)
    stream_wide = residual_entry_input.astype(jnp.float32) + mixed_rows
    stream = stream_wide.astype(jnp.bfloat16)
    stream_wide = lax.optimization_barrier(stream).astype(jnp.float32)
    normed_rows = (
        stream_wide
        * lax.rsqrt(jnp.mean(stream_wide * stream_wide, axis=-1, keepdims=True) + eps)
        * feedforward_norm_gain[None, :]
    ).astype(jnp.bfloat16)
    group_rows = lax.all_gather(normed_rows, "tp", axis=0, tiled=True)
    earlier_rows = shifted(group_rows[-2:], "sp", 1)
    window = jnp.concatenate([earlier_rows, group_rows], axis=0)
    up_gate = jnp.dot(
        window,
        lax.all_gather(gate_up_weight, "sp", axis=0, tiled=True),
        preferred_element_type=jnp.float32,
    )
    up_value = jnp.dot(
        window,
        lax.all_gather(value_up_weight, "sp", axis=0, tiled=True),
        preferred_element_type=jnp.float32,
    )
    conv_g = (
        gate_filter_taps[0][None, :] * up_gate[:-2]
        + gate_filter_taps[1][None, :] * up_gate[1:-1]
        + gate_filter_taps[2][None, :] * up_gate[2:]
    )
    conv_v = (
        value_filter_taps[0][None, :] * up_value[:-2]
        + value_filter_taps[1][None, :] * up_value[1:-1]
        + value_filter_taps[2][None, :] * up_value[2:]
    )
    hidden = (jax.nn.silu(conv_g) * conv_v).astype(jnp.bfloat16)
    whole_down = lax.all_gather(down_projection_weight, "sp", axis=1, tiled=True)
    ffn_rows = lax.psum_scatter(
        jnp.dot(hidden, whole_down, preferred_element_type=jnp.float32).astype(jnp.bfloat16),
        "tp",
        scatter_dimension=0,
        tiled=True,
    ).astype(jnp.float32)
    return (stream_wide + ffn_rows).astype(jnp.bfloat16)


def solution(mesh):
    in_specs = (
        P(("sp", "tp"), None),
        P("sp", "tp"),
        P("sp", "tp"),
        P("sp", "tp"),
        P("sp", "tp"),
        P("sp", "tp"),
        P("sp", "tp"),
        P("sp", "tp"),
        P("tp", None),
        P("tp", None),
        P(),
        P("sp", "tp"),
        P("sp", "tp"),
        P(None, "tp"),
        P(None, "tp"),
        P("tp", "sp"),
    )
    out_specs = P(("sp", "tp"), None)
    return jax.shard_map(local, mesh=mesh, in_specs=in_specs, out_specs=out_specs, check_vma=False)
```

profile of v0, /device:TPU:0, one launch (start us, length us, event | category | flops | bytes accessed | tf_op | source)
XLA Modules:
  0.0 629.0 jit_solution(18224603662122398015)
XLA Ops:
  7.6 1.3 reshape.215
  9.9 2.0 reshape.216
  12.8 105.2 %while.39 = (s32[]{:T(128)}, f32[2,256,128]{2,1,0:T(8,128)S(1)}, f32[2,128]{1,0:T(2,128)S(1)}, f32[2]{0:T(128)S(1)}, f32[8,128,2,256]{1,0,3,2:T(8,128)}, /*index...) while((s32[]{:T(128)}, f32[2,256,128]{2,1,0:T(8,128)S(1)}, ...), condition=%wide.region_6.7_spmd.clone, body=%wide.region_0.6_spmd.clone.sunk | while | flops 144166400 | bytes 4685610 | solution.py:144
  17.3 8.2 %dynamic_update_slice.19 = f32[8,128,2,256]{1,0,3,2:T(8,128)} dynamic-update-slice(f32[8,128,2,256]{1,0,3,2:T(8,128)} %get-tuple-element.661, f32[1,128,2,256]{1,0,3,2:T(1,128)S(1)} %copy.248, s32[]{:T(128)} %get-tuple-element.657, s32[]{:T(128)} %constant.83.clone.1..sunk, s32[]{:T(128)} %constant.83.clone.1..sunk, s32[]{:T(128)} %constant.83.clone.1..sunk) | dynamic-update-slice | bytes 524292 | tf_op jit(solution)/shard_map/while/body/jit(dynamic_update_index_in_dim)/dynamic_update_slice | solution.py:144
  30.5 8.2 %dynamic_update_slice.19 = f32[8,128,2,256]{1,0,3,2:T(8,128)} dynamic-update-slice(f32[8,128,2,256]{1,0,3,2:T(8,128)} %get-tuple-element.661, f32[1,128,2,256]{1,0,3,2:T(1,128)S(1)} %copy.248, s32[]{:T(128)} %get-tuple-element.657, s32[]{:T(128)} %constant.83.clone.1..sunk, s32[]{:T(128)} %constant.83.clone.1..sunk, s32[]{:T(128)} %constant.83.clone.1..sunk) | dynamic-update-slice | bytes 524292 | tf_op jit(solution)/shard_map/while/body/jit(dynamic_update_index_in_dim)/dynamic_update_slice | solution.py:144
  43.7 8.2 %dynamic_update_slice.19 = f32[8,128,2,256]{1,0,3,2:T(8,128)} dynamic-update-slice(f32[8,128,2,256]{1,0,3,2:T(8,128)} %get-tuple-element.661, f32[1,128,2,256]{1,0,3,2:T(1,128)S(1)} %copy.248, s32[]{:T(128)} %get-tuple-element.657, s32[]{:T(128)} %constant.83.clone.1..sunk, s32[]{:T(128)} %constant.83.clone.1..sunk, s32[]{:T(128)} %constant.83.clone.1..sunk) | dynamic-update-slice | bytes 524292 | tf_op jit(solution)/shard_map/while/body/jit(dynamic_update_index_in_dim)/dynamic_update_slice | solution.py:144
  56.8 8.2 %dynamic_update_slice.19 = f32[8,128,2,256]{1,0,3,2:T(8,128)} dynamic-update-slice(f32[8,128,2,256]{1,0,3,2:T(8,128)} %get-tuple-element.661, f32[1,128,2,256]{1,0,3,2:T(1,128)S(1)} %copy.248, s32[]{:T(128)} %get-tuple-element.657, s32[]{:T(128)} %constant.83.clone.1..sunk, s32[]{:T(128)} %constant.83.clone.1..sunk, s32[]{:T(128)} %constant.83.clone.1..sunk) | dynamic-update-slice | bytes 524292 | tf_op jit(solution)/shard_map/while/body/jit(dynamic_update_index_in_dim)/dynamic_update_slice | solution.py:144
  70.0 8.2 %dynamic_update_slice.19 = f32[8,128,2,256]{1,0,3,2:T(8,128)} dynamic-update-slice(f32[8,128,2,256]{1,0,3,2:T(8,128)} %get-tuple-element.661, f32[1,128,2,256]{1,0,3,2:T(1,128)S(1)} %copy.248, s32[]{:T(128)} %get-tuple-element.657, s32[]{:T(128)} %constant.83.clone.1..sunk, s32[]{:T(128)} %constant.83.clone.1..sunk, s32[]{:T(128)} %constant.83.clone.1..sunk) | dynamic-update-slice | bytes 524292 | tf_op jit(solution)/shard_map/while/body/jit(dynamic_update_index_in_dim)/dynamic_update_slice | solution.py:144
  83.1 8.2 %dynamic_update_slice.19 = f32[8,128,2,256]{1,0,3,2:T(8,128)} dynamic-update-slice(f32[8,128,2,256]{1,0,3,2:T(8,128)} %get-tuple-element.661, f32[1,128,2,256]{1,0,3,2:T(1,128)S(1)} %copy.248, s32[]{:T(128)} %get-tuple-element.657, s32[]{:T(128)} %constant.83.clone.1..sunk, s32[]{:T(128)} %constant.83.clone.1..sunk, s32[]{:T(128)} %constant.83.clone.1..sunk) | dynamic-update-slice | bytes 524292 | tf_op jit(solution)/shard_map/while/body/jit(dynamic_update_index_in_dim)/dynamic_update_slice | solution.py:144
  96.3 8.2 %dynamic_update_slice.19 = f32[8,128,2,256]{1,0,3,2:T(8,128)} dynamic-update-slice(f32[8,128,2,256]{1,0,3,2:T(8,128)} %get-tuple-element.661, f32[1,128,2,256]{1,0,3,2:T(1,128)S(1)} %copy.248, s32[]{:T(128)} %get-tuple-element.657, s32[]{:T(128)} %constant.83.clone.1..sunk, s32[]{:T(128)} %constant.83.clone.1..sunk, s32[]{:T(128)} %constant.83.clone.1..sunk) | dynamic-update-slice | bytes 524292 | tf_op jit(solution)/shard_map/while/body/jit(dynamic_update_index_in_dim)/dynamic_update_slice | solution.py:144
  109.4 8.2 %dynamic_update_slice.19 = f32[8,128,2,256]{1,0,3,2:T(8,128)} dynamic-update-slice(f32[8,128,2,256]{1,0,3,2:T(8,128)} %get-tuple-element.661, f32[1,128,2,256]{1,0,3,2:T(1,128)S(1)} %copy.248, s32[]{:T(128)} %get-tuple-element.657, s32[]{:T(128)} %constant.83.clone.1..sunk, s32[]{:T(128)} %constant.83.clone.1..sunk, s32[]{:T(128)} %constant.83.clone.1..sunk) | dynamic-update-slice | bytes 524292 | tf_op jit(solution)/shard_map/while/body/jit(dynamic_update_index_in_dim)/dynamic_update_slice | solution.py:144
  122.2 22.3 %all-gather.3 = bf16[8,1,2]{2,1,0:T(2,128)(2,1)S(1)} all-gather(bf16[1,1,2]{2,1,0:T(2,128)(2,1)S(1)} %bitcast.273), channel_id=1, replica_groups=mesh['sp'=8,'tp'=4] {'sp'}, dimensions={0}, use_global_device_ids=true | all-gather | bytes 36 | tf_op jit(solution)/shard_map/all_gather | solution.py:14
  144.5 17.5 %all-reduce = bf16[16]{0:T(256)(128)(2,1)S(1)} all-reduce(bf16[16]{0:T(256)(128)(2,1)S(1)} %dynamic-update-slice), channel_id=2, replica_groups=mesh['sp'=8,'tp'=4] {'sp'}, use_global_device_ids=true, to_apply=%add | all-reduce | flops 16 | bytes 64
  163.5 1.3 copy.156
  164.8 1.7 reshape.187
  166.5 18.0 %all-gather.4 = bf16[8,2,128]{2,1,0:T(2,128)(2,1)S(1)} all-gather(bf16[1,2,128]{2,1,0:T(2,128)(2,1)S(1)} %convert_bitcast_fusion), channel_id=4, replica_groups=mesh['sp'=8,'tp'=4] {'sp'}, dimensions={0}, use_global_device_ids=true | all-gather | bytes 4608 | tf_op jit(solution)/shard_map/all_gather | solution.py:14
  184.5 10.5 %while.40 = (s32[]{:T(128)}, f32[2,256,128]{2,1,0:T(8,128)S(1)}, f32[2,128]{1,0:T(2,128)S(1)}, f32[2]{0:T(128)S(1)}, s32[]{:T(128)}, /*index=5*/bf16[8,2]{0,1:T(...) while((s32[]{:T(128)}, f32[2,256,128]{2,1,0:T(8,128)S(1)}, ...), condition=%wide.region_10.11_spmd.clone, body=%wide.region_9.10_spmd.clone.sunk | while | flops 394772 | bytes 658157 | solution.py:29
  196.2 2.2 multiply_reduce_fusion
  198.7 1.9 copy.141
  200.6 2.5 multiply_convert_fusion
  203.1 26.9 %all_to_all.19 = bf16[4,256,512]{2,1,0:T(8,128)(2,1)S(1)} all-to-all(bf16[4,256,512]{2,1,0:T(8,128)(2,1)S(1)} %bitcast.262), channel_id=1, replica_groups=mesh['sp'=8,'tp'=4] {'tp'}, dimensions={0} | all-to-all | bytes 2097152 | tf_op jit(solution)/shard_map/all_to_all | solution.py:191
  230.5 5.7 fusion.45
  239.9 33.9 %all-gather.14.cloned.1.call-done = bf16[1024,2048]{1,0:T(8,128)(2,1)} async-done(((bf16[256,2048]{1,0:T(8,128)(2,1)}), bf16[1024,2048]{1,0:T(8,128)(2,1)}) %all-gather.14.cloned.1.call-update) | async-done | bytes 4194320 | tf_op jit(solution)/shard_map/all_gather | solution.py:201
  274.6 3.4 collective-permute-start
  278.1 90.1 %all-gather.16.cloned.1.call-done = bf16[2048,1408]{1,0:T(8,128)(2,1)} async-done(((bf16[256,1408]{1,0:T(8,128)(2,1)}), bf16[2048,1408]{1,0:T(8,128)(2,1)}) %all-gather.16.cloned.1.call-update) | async-done | bytes 5767184 | tf_op jit(solution)/shard_map/all_gather | solution.py:206
  368.2 11.9 %fusion.44 = f32[1026,1408]{1,0:T(8,128)} fusion(bf16[2048,1408]{1,0:T(8,128)(2,1)} %all-gather.16.cloned.1.call-done, bf16[1024,2048]{1,0:T(8,128)(2,1)} %all-gather.14.cloned.1.call-done, bf16[2,2048]{1,0:T(2,128)(2,1)S(1)} %collective-permute-done), kind=kOutput, calls=%fused_computation.90 | convolution fusion | flops 5925519360 | bytes 15748096 | tf_op jit(solution)/shard_map/dot_general | solution.py:204
  380.1 80.6 %all-gather.18.cloned.1.call-done = bf16[2048,1408]{1,0:T(8,128)(2,1)} async-done(((bf16[256,1408]{1,0:T(8,128)(2,1)}), bf16[2048,1408]{1,0:T(8,128)(2,1)}) %all-gather.18.cloned.1.call-update) | async-done | bytes 5767184 | tf_op jit(solution)/shard_map/all_gather | solution.py:211
  460.7 11.9 %fusion.43 = f32[1026,1408]{1,0:T(8,128)} fusion(bf16[2048,1408]{1,0:T(8,128)(2,1)} %all-gather.18.cloned.1.call-done, bf16[1024,2048]{1,0:T(8,128)(2,1)} %all-gather.14.cloned.1.call-done, bf16[2,2048]{1,0:T(2,128)(2,1)S(1)} %collective-permute-done), kind=kOutput, calls=%fused_computation.89 | convolution fusion | flops 5925519360 | bytes 15748096 | tf_op jit(solution)/shard_map/dot_general | solution.py:209
  472.6 81.3 %all-gather.20.cloned.1.call-done = bf16[1408,2048]{1,0:T(8,128)(2,1)} async-done(((bf16[1408,256]{1,0:T(8,128)(2,1)}), bf16[1408,2048]{1,0:T(8,128)(2,1)}) %all-gather.20.cloned.1.call-update) | async-done | bytes 5767184 | tf_op jit(solution)/shard_map/all_gather | solution.py:225
  554.0 22.7 %convolution_convert_fusion = bf16[1024,2048]{1,0:T(8,128)(2,1)} fusion(bf16[1408,2048]{1,0:T(8,128)(2,1)} %all-gather.20.cloned.1.call-done, f32[1026,1408]{1,0:T(8,128)} %fusion.43, f32[1026,1408]{1,0:T(8,128)} %fusion.44, f32[1408]{0:T(1024)S(1)} %get-tuple-element.403, f32[1408]{0:T(1024)S(1)} %get-tuple-element.404, f32[1408]{0:T(1024)S(1)} %get-tuple-element.402, ...), kind=kOutput, calls=%fused_computation.85 | convolution fusion | flops 5930745856 | bytes 44598272 | tf_op jit(solution)/shard_map/dot_general | solution.py:227
  576.7 42.9 %reduce-scatter.2.cloned.1.call-done = bf16[256,2048]{1,0:T(8,128)(2,1)} async-done(((bf16[1024,2048]{1,0:T(8,128)(2,1)}), bf16[256,2048]{1,0:T(8,128)(2,1)}) %reduce-scatter.2.cloned.1.call-update) | async-done | bytes 1048592 | tf_op jit(solution)/shard_map/reduce_scatter | solution.py:226
  619.6 2.6 fusion.49
  (337 shorter events, 63.3 us)
Async XLA Ops:
  6.5 5.3 copy-start.1
  6.5 178.0 %all-gather.22.cloned.1.call-start = ((), (), s32[]{:S(2)}) async-start(), calls=%async_computation.8 | async-start | bytes 1179648 | tf_op jit(solution)/shard_map/all_gather | solution.py:14
  12.8 107.7 %copy-start.7 = (u32[32]{0:T(128)S(1)}, u32[32]{0:T(128)}, u32[]{:S(2)}) copy-start(u32[32]{0:T(128)} %constant.101) | copy-start | bytes 388
  118.7 111.8 %all-gather.12.cloned.1.call-start = ((), (), s32[]{:S(2)}) async-start(), calls=%async_computation.2 | async-start | bytes 10485760 | tf_op jit(solution)/shard_map/all_gather | solution.py:190
  119.4 154.4 %all-gather.14.cloned.1.call-start = ((), (), s32[]{:S(2)}) async-start(), calls=%async_computation.3 | async-start | bytes 5242880 | tf_op jit(solution)/shard_map/all_gather | solution.py:201
  163.5 31.6 %copy-start.2 = (bf16[1024,256]{1,0:T(8,128)(2,1)S(1)}, bf16[1024,256]{1,0:T(8,128)(2,1)}, u32[]{:S(2)}) copy-start(bf16[1024,256]{1,0:T(8,128)(2,1)} %param.21) | copy-start | bytes 1572868
  196.2 2.3 copy-start.6
  200.6 29.9 %copy-start = (bf16[256,2048]{1,0:T(8,128)(2,1)S(1)}, bf16[256,2048]{1,0:T(8,128)(2,1)}, u32[]{:S(2)}) copy-start(bf16[256,2048]{1,0:T(8,128)(2,1)} %param.20) | copy-start | bytes 3145732
  230.5 6.1 copy-start.5
  236.3 41.7 %copy-start.3 = (f32[3,1408]{1,0:T(4,128)S(1)}, f32[3,1408]{1,0:T(4,128)}, u32[]{:S(2)}) copy-start(f32[3,1408]{1,0:T(4,128)} %param.34) | copy-start | bytes 50692
  236.3 41.7 %copy-start.4 = (f32[3,1408]{1,0:T(4,128)S(1)}, f32[3,1408]{1,0:T(4,128)}, u32[]{:S(2)}) copy-start(f32[3,1408]{1,0:T(4,128)} %param.33) | copy-start | bytes 50692
  237.9 130.3 %all-gather.16.cloned.1.call-start = ((), (), s32[]{:S(2)}) async-start(), calls=%async_computation.4 | async-start | bytes 6488064 | tf_op jit(solution)/shard_map/all_gather | solution.py:206
  238.5 222.3 %all-gather.18.cloned.1.call-start = ((), (), s32[]{:S(2)}) async-start(), calls=%async_computation.5 | async-start | bytes 6488064 | tf_op jit(solution)/shard_map/all_gather | solution.py:211
  239.1 314.9 %all-gather.20.cloned.1.call-start = ((), (), s32[]{:S(2)}) async-start(), calls=%async_computation.6 | async-start | bytes 6488064 | tf_op jit(solution)/shard_map/all_gather | solution.py:225
  239.7 379.9 %reduce-scatter.2.cloned.1.call-start = ((), (), s32[]{:S(2)}) async-start(), calls=%async_computation.7 | async-start | bytes 5242880 | tf_op jit(solution)/shard_map/reduce_scatter | solution.py:226
  274.6 93.6 %collective-permute-start = (bf16[2,2048]{1,0:T(2,128)(2,1)S(1)}, bf16[2,2048]{1,0:T(2,128)(2,1)S(1)}, u32[]{:S(2)}, u32[]{:S(2)}) collective-permute-start(bf16[2,2048]{1,0:T(2,128)(2,1)S(1)} %slice.72), channel_id=1, source_target_pairs={{0,4},{4,8},{8,12},{12,16},{16,20},{20,24},{24,28},{1,5},{5,9},{9,... | collective-permute-start | bytes 24584 | tf_op jit(solution)/shard_map/ppermute | solution.py:35
Sparse Core Ops, SparseCore 0:
  118.8 43.2 all-gather.21
  163.6 66.6 all-gather.11
  238.0 35.7 all-gather.13
  275.8 92.3 all-gather.15
  370.2 90.4 all-gather.17
  462.6 91.2 all-gather.19
  576.8 42.7 reduce-scatter.1
where the time goes:
time: 631 us; the launch traced here: 629 us
  waiting for transfers between devices  331 us (52%)
  local copies, waits for them, and re-layouts  97.1 us (15%)
  blocking collectives  84.7 us (13%)
  matrix products  67.5 us (11%)
  other arithmetic  29.4 us (5%)
  between operations  14.4 us (2%)
    all_gather x1, waiting for transfers between devices, local(): lax.all_gather(gate_up_weight, 'sp', axis=0, tiled=True)  90.1 us
    all_gather x1, waiting for transfers between devices, local(): lax.all_gather(down_projection_weight, 'sp', axis=1, tiled=True)  81.3 us
    all_gather x1, waiting for transfers between devices, local(): lax.all_gather(value_up_weight, 'sp', axis=0, tiled=True)  80.6 us
    dynamic_update_slice x16, local copies, waits for them, and re-layouts, local(): lax.scan(local_step, initial, (blocks(queries_low), blocks(keys_low), blo...  66.7 us
    reduce_scatter x1, waiting for transfers between devices, local(): lax.psum_scatter(jnp.dot(hidden, whole_down, preferred_element_type=jnp.f...  42.9 us
    all_gather x2, blocking collectives, carried_in(): lax.all_gather(part.astype(kind), axis)  40.3 us
    all_gather x1, waiting for transfers between devices, local(): group_rows = lax.all_gather(normed_rows, 'tp', axis=0, tiled=True)  33.9 us
    all_to_all x1, blocking collectives, local(): lax.all_to_all(gated_rows, 'tp', split_axis=0, concat_axis=1, tiled=True)  26.9 us
  transfers between devices with their start and end apart: 8, of which 5 were waited for; matrix products, arithmetic and copies ran while one was open for 8% of the time, Pallas kernels for 0%

commit v1 on v0

--- a/solution.py
+++ b/solution.py
@@ -198,7 +198,9 @@
         * lax.rsqrt(jnp.mean(stream_wide * stream_wide, axis=-1, keepdims=True) + eps)
         * feedforward_norm_gain[None, :]
     ).astype(jnp.bfloat16)
-    group_rows = lax.all_gather(normed_rows, "tp", axis=0, tiled=True)
+    group_rows = jnp.concatenate(
+        lax.all_to_all(jnp.stack([normed_rows] * lax.axis_size("tp")), "tp", 0, 0), axis=0
+    )
     earlier_rows = shifted(group_rows[-2:], "sp", 1)
     window = jnp.concatenate([earlier_rows, group_rows], axis=0)
     up_gate = jnp.dot(

time: 631 us -> 590 us (0.935)
  waiting for transfers between devices: 331 us -> 239 us
  blocking collectives: 84.7 us -> 136 us
    all_gather x1, waiting for transfers between devices: 90.1 us -> 31.5 us  [local(): lax.all_gather(gate_up_weight, 'sp', axis=0, tiled=True)]
    all_to_all x0 -> x1, blocking collectives: none -> 50.8 us  [local(): lax.all_to_all(jnp.stack([normed_rows] * lax.axis_size('tp')), 'tp', 0, 0)]
    all_gather x1 -> x0, waiting for transfers between devices: 33.9 us -> none  [local(): group_rows = lax.all_gather(normed_rows, 'tp', axis=0, tiled=True)]
  transfers between devices with their start and end apart: 8 -> 7, of which waited for: 5 -> 4; matrix products, arithmetic and copies ran while one was open for 8% -> 9% of each run, Pallas kernels for 0% -> 0%
where the time goes in v1:
time: 590 us; the launch traced here: 587 us
  waiting for transfers between devices  239 us (41%)
  blocking collectives  136 us (23%)
  local copies, waits for them, and re-layouts  96.7 us (16%)
  matrix products  67.4 us (11%)
  other arithmetic  28.4 us (5%)
  between operations  14.4 us (2%)
    all_gather x1, waiting for transfers between devices, local(): lax.all_gather(down_projection_weight, 'sp', axis=1, tiled=True)  81.3 us
    all_gather x1, waiting for transfers between devices, local(): lax.all_gather(value_up_weight, 'sp', axis=0, tiled=True)  80.7 us
    dynamic_update_slice x16, local copies, waits for them, and re-layouts, local(): lax.scan(local_step, initial, (blocks(queries_low), blocks(keys_low), blo...  66.7 us
    all_to_all x1, blocking collectives, local(): lax.all_to_all(jnp.stack([normed_rows] * lax.axis_size('tp')), 'tp', 0, 0)  50.8 us
    reduce_scatter x1, waiting for transfers between devices, local(): lax.psum_scatter(jnp.dot(hidden, whole_down, preferred_element_type=jnp.f...  42.9 us
    all_gather x2, blocking collectives, carried_in(): lax.all_gather(part.astype(kind), axis)  34.7 us
    all_gather x1, waiting for transfers between devices, local(): lax.all_gather(gate_up_weight, 'sp', axis=0, tiled=True)  31.5 us
    all_to_all x1, blocking collectives, local(): lax.all_to_all(gated_rows, 'tp', split_axis=0, concat_axis=1, tiled=True)  26.9 us
  transfers between devices with their start and end apart: 7, of which 4 were waited for; matrix products, arithmetic and copies ran while one was open for 9% of the time, Pallas kernels for 0%

profile of v1, /device:TPU:0, one launch (start us, length us, event | category | flops | bytes accessed | tf_op | source)
XLA Modules:
  0.0 587.2 jit_solution(6658395831791031615)
XLA Ops:
  7.6 1.3 reshape.221
  9.9 2.0 reshape.222
  12.8 105.2 %while.39 = (s32[]{:T(128)}, f32[2,256,128]{2,1,0:T(8,128)S(1)}, f32[2,128]{1,0:T(2,128)S(1)}, f32[2]{0:T(128)S(1)}, f32[8,128,2,256]{1,0,3,2:T(8,128)}, /*index...) while((s32[]{:T(128)}, f32[2,256,128]{2,1,0:T(8,128)S(1)}, ...), condition=%wide.region_6.7_spmd.clone, body=%wide.region_0.6_spmd.clone.sunk | while | flops 144166400 | bytes 4685610 | solution.py:144
  17.3 8.2 %dynamic_update_slice.19 = f32[8,128,2,256]{1,0,3,2:T(8,128)} dynamic-update-slice(f32[8,128,2,256]{1,0,3,2:T(8,128)} %get-tuple-element.661, f32[1,128,2,256]{1,0,3,2:T(1,128)S(1)} %copy.248, s32[]{:T(128)} %get-tuple-element.657, s32[]{:T(128)} %constant.83.clone.1..sunk, s32[]{:T(128)} %constant.83.clone.1..sunk, s32[]{:T(128)} %constant.83.clone.1..sunk) | dynamic-update-slice | bytes 524292 | tf_op jit(solution)/shard_map/while/body/jit(dynamic_update_index_in_dim)/dynamic_update_slice | solution.py:144
  30.5 8.2 %dynamic_update_slice.19 = f32[8,128,2,256]{1,0,3,2:T(8,128)} dynamic-update-slice(f32[8,128,2,256]{1,0,3,2:T(8,128)} %get-tuple-element.661, f32[1,128,2,256]{1,0,3,2:T(1,128)S(1)} %copy.248, s32[]{:T(128)} %get-tuple-element.657, s32[]{:T(128)} %constant.83.clone.1..sunk, s32[]{:T(128)} %constant.83.clone.1..sunk, s32[]{:T(128)} %constant.83.clone.1..sunk) | dynamic-update-slice | bytes 524292 | tf_op jit(solution)/shard_map/while/body/jit(dynamic_update_index_in_dim)/dynamic_update_slice | solution.py:144
  43.6 8.2 %dynamic_update_slice.19 = f32[8,128,2,256]{1,0,3,2:T(8,128)} dynamic-update-slice(f32[8,128,2,256]{1,0,3,2:T(8,128)} %get-tuple-element.661, f32[1,128,2,256]{1,0,3,2:T(1,128)S(1)} %copy.248, s32[]{:T(128)} %get-tuple-element.657, s32[]{:T(128)} %constant.83.clone.1..sunk, s32[]{:T(128)} %constant.83.clone.1..sunk, s32[]{:T(128)} %constant.83.clone.1..sunk) | dynamic-update-slice | bytes 524292 | tf_op jit(solution)/shard_map/while/body/jit(dynamic_update_index_in_dim)/dynamic_update_slice | solution.py:144
  56.8 8.2 %dynamic_update_slice.19 = f32[8,128,2,256]{1,0,3,2:T(8,128)} dynamic-update-slice(f32[8,128,2,256]{1,0,3,2:T(8,128)} %get-tuple-element.661, f32[1,128,2,256]{1,0,3,2:T(1,128)S(1)} %copy.248, s32[]{:T(128)} %get-tuple-element.657, s32[]{:T(128)} %constant.83.clone.1..sunk, s32[]{:T(128)} %constant.83.clone.1..sunk, s32[]{:T(128)} %constant.83.clone.1..sunk) | dynamic-update-slice | bytes 524292 | tf_op jit(solution)/shard_map/while/body/jit(dynamic_update_index_in_dim)/dynamic_update_slice | solution.py:144
  70.0 8.2 %dynamic_update_slice.19 = f32[8,128,2,256]{1,0,3,2:T(8,128)} dynamic-update-slice(f32[8,128,2,256]{1,0,3,2:T(8,128)} %get-tuple-element.661, f32[1,128,2,256]{1,0,3,2:T(1,128)S(1)} %copy.248, s32[]{:T(128)} %get-tuple-element.657, s32[]{:T(128)} %constant.83.clone.1..sunk, s32[]{:T(128)} %constant.83.clone.1..sunk, s32[]{:T(128)} %constant.83.clone.1..sunk) | dynamic-update-slice | bytes 524292 | tf_op jit(solution)/shard_map/while/body/jit(dynamic_update_index_in_dim)/dynamic_update_slice | solution.py:144
  83.1 8.2 %dynamic_update_slice.19 = f32[8,128,2,256]{1,0,3,2:T(8,128)} dynamic-update-slice(f32[8,128,2,256]{1,0,3,2:T(8,128)} %get-tuple-element.661, f32[1,128,2,256]{1,0,3,2:T(1,128)S(1)} %copy.248, s32[]{:T(128)} %get-tuple-element.657, s32[]{:T(128)} %constant.83.clone.1..sunk, s32[]{:T(128)} %constant.83.clone.1..sunk, s32[]{:T(128)} %constant.83.clone.1..sunk) | dynamic-update-slice | bytes 524292 | tf_op jit(solution)/shard_map/while/body/jit(dynamic_update_index_in_dim)/dynamic_update_slice | solution.py:144
  96.3 8.2 %dynamic_update_slice.19 = f32[8,128,2,256]{1,0,3,2:T(8,128)} dynamic-update-slice(f32[8,128,2,256]{1,0,3,2:T(8,128)} %get-tuple-element.661, f32[1,128,2,256]{1,0,3,2:T(1,128)S(1)} %copy.248, s32[]{:T(128)} %get-tuple-element.657, s32[]{:T(128)} %constant.83.clone.1..sunk, s32[]{:T(128)} %constant.83.clone.1..sunk, s32[]{:T(128)} %constant.83.clone.1..sunk) | dynamic-update-slice | bytes 524292 | tf_op jit(solution)/shard_map/while/body/jit(dynamic_update_index_in_dim)/dynamic_update_slice | solution.py:144
  109.4 8.2 %dynamic_update_slice.19 = f32[8,128,2,256]{1,0,3,2:T(8,128)} dynamic-update-slice(f32[8,128,2,256]{1,0,3,2:T(8,128)} %get-tuple-element.661, f32[1,128,2,256]{1,0,3,2:T(1,128)S(1)} %copy.248, s32[]{:T(128)} %get-tuple-element.657, s32[]{:T(128)} %constant.83.clone.1..sunk, s32[]{:T(128)} %constant.83.clone.1..sunk, s32[]{:T(128)} %constant.83.clone.1..sunk) | dynamic-update-slice | bytes 524292 | tf_op jit(solution)/shard_map/while/body/jit(dynamic_update_index_in_dim)/dynamic_update_slice | solution.py:144
  123.0 23.3 %all-reduce = bf16[16]{0:T(256)(128)(2,1)S(1)} all-reduce(bf16[16]{0:T(256)(128)(2,1)S(1)} %dynamic-update-slice), channel_id=2, replica_groups=mesh['sp'=8,'tp'=4] {'sp'}, use_global_device_ids=true, to_apply=%add | all-reduce | flops 16 | bytes 64
  146.3 16.4 %all-gather.4 = bf16[8,2,128]{2,1,0:T(2,128)(2,1)S(1)} all-gather(bf16[1,2,128]{2,1,0:T(2,128)(2,1)S(1)} %convert_bitcast_fusion), channel_id=4, replica_groups=mesh['sp'=8,'tp'=4] {'sp'}, dimensions={0}, use_global_device_ids=true | all-gather | bytes 4608 | tf_op jit(solution)/shard_map/all_gather | solution.py:14
  163.9 18.3 %all-gather.3 = bf16[8,1,2]{2,1,0:T(2,128)(2,1)S(1)} all-gather(bf16[1,1,2]{2,1,0:T(2,128)(2,1)S(1)} %bitcast.279), channel_id=1, replica_groups=mesh['sp'=8,'tp'=4] {'sp'}, dimensions={0}, use_global_device_ids=true | all-gather | bytes 36 | tf_op jit(solution)/shard_map/all_gather | solution.py:14
  182.7 1.7 reshape.192
  184.4 10.5 %while.40 = (s32[]{:T(128)}, f32[2,256,128]{2,1,0:T(8,128)S(1)}, f32[2,128]{1,0:T(2,128)S(1)}, f32[2]{0:T(128)S(1)}, s32[]{:T(128)}, /*index=5*/bf16[8,2]{0,1:T(...) while((s32[]{:T(128)}, f32[2,256,128]{2,1,0:T(8,128)S(1)}, ...), condition=%wide.region_10.11_spmd.clone, body=%wide.region_9.10_spmd.clone.sunk | while | flops 394772 | bytes 658157 | solution.py:29
  196.1 2.2 multiply_reduce_fusion
  198.6 1.9 copy.141
  200.5 2.5 multiply_convert_fusion
  203.0 26.9 %all_to_all.24 = bf16[4,256,512]{2,1,0:T(8,128)(2,1)S(1)} all-to-all(bf16[4,256,512]{2,1,0:T(8,128)(2,1)S(1)} %bitcast.266), channel_id=1, replica_groups=mesh['sp'=8,'tp'=4] {'tp'}, dimensions={0} | all-to-all | bytes 2097152 | tf_op jit(solution)/shard_map/all_to_all | solution.py:191
  230.5 5.7 fusion.45
  237.4 50.8 %all_to_all.25 = bf16[4,256,2048]{2,1,0:T(8,128)(2,1)S(1)} all-to-all(bf16[4,256,2048]{2,1,0:T(8,128)(2,1)S(1)} %stack.2), channel_id=1, replica_groups=mesh['sp'=8,'tp'=4] {'tp'}, dimensions={0} | all-to-all | bytes 8388608 | tf_op jit(solution)/shard_map/all_to_all | solution.py:202
  288.2 2.0 copy-done
  290.2 4.6 collective-permute-start
  294.9 31.5 %all-gather.13.cloned.1.call-done = bf16[2048,1408]{1,0:T(8,128)(2,1)} async-done(((bf16[256,1408]{1,0:T(8,128)(2,1)}), bf16[2048,1408]{1,0:T(8,128)(2,1)}) %all-gather.13.cloned.1.call-update) | async-done | bytes 5767184 | tf_op jit(solution)/shard_map/all_gather | solution.py:208
  326.4 11.9 %fusion.44 = f32[1026,1408]{1,0:T(8,128)} fusion(bf16[2048,1408]{1,0:T(8,128)(2,1)} %all-gather.13.cloned.1.call-done, bf16[1024,2048]{1,0:T(8,128)(2,1)} %bitcast.263, bf16[2,2048]{1,0:T(2,128)(2,1)S(1)} %collective-permute-done), kind=kOutput, calls=%fused_computation.90 | convolution fusion | flops 5925519360 | bytes 15748096 | tf_op jit(solution)/shard_map/dot_general | solution.py:206
  338.3 80.7 %all-gather.15.cloned.1.call-done = bf16[2048,1408]{1,0:T(8,128)(2,1)} async-done(((bf16[256,1408]{1,0:T(8,128)(2,1)}), bf16[2048,1408]{1,0:T(8,128)(2,1)}) %all-gather.15.cloned.1.call-update) | async-done | bytes 5767184 | tf_op jit(solution)/shard_map/all_gather | solution.py:213
  419.0 11.9 %fusion.43 = f32[1026,1408]{1,0:T(8,128)} fusion(bf16[2048,1408]{1,0:T(8,128)(2,1)} %all-gather.15.cloned.1.call-done, bf16[1024,2048]{1,0:T(8,128)(2,1)} %bitcast.264, bf16[2,2048]{1,0:T(2,128)(2,1)S(1)} %collective-permute-done), kind=kOutput, calls=%fused_computation.89 | convolution fusion | flops 5925519360 | bytes 15748096 | tf_op jit(solution)/shard_map/dot_general | solution.py:211
  430.9 81.3 %all-gather.17.cloned.1.call-done = bf16[1408,2048]{1,0:T(8,128)(2,1)} async-done(((bf16[1408,256]{1,0:T(8,128)(2,1)}), bf16[1408,2048]{1,0:T(8,128)(2,1)}) %all-gather.17.cloned.1.call-update) | async-done | bytes 5767184 | tf_op jit(solution)/shard_map/all_gather | solution.py:227
  512.2 22.7 %convolution_convert_fusion = bf16[1024,2048]{1,0:T(8,128)(2,1)} fusion(bf16[1408,2048]{1,0:T(8,128)(2,1)} %all-gather.17.cloned.1.call-done, f32[1026,1408]{1,0:T(8,128)} %fusion.43, f32[1026,1408]{1,0:T(8,128)} %fusion.44, f32[1408]{0:T(1024)S(1)} %get-tuple-element.403, f32[1408]{0:T(1024)S(1)} %get-tuple-element.404, f32[1408]{0:T(1024)S(1)} %get-tuple-element.402, ...), kind=kOutput, calls=%fused_computation.85 | convolution fusion | flops 5930745856 | bytes 44598272 | tf_op jit(solution)/shard_map/dot_general | solution.py:229
  534.9 42.9 %reduce-scatter.2.cloned.1.call-done = bf16[256,2048]{1,0:T(8,128)(2,1)} async-done(((bf16[1024,2048]{1,0:T(8,128)(2,1)}), bf16[256,2048]{1,0:T(8,128)(2,1)}) %reduce-scatter.2.cloned.1.call-update) | async-done | bytes 1048592 | tf_op jit(solution)/shard_map/reduce_scatter | solution.py:228
  577.8 2.6 fusion.49
  (342 shorter events, 61.2 us)
Async XLA Ops:
  6.5 5.3 copy-start.2
  6.5 177.9 %all-gather.19.cloned.1.call-start = ((), (), s32[]{:S(2)}) async-start(), calls=%async_computation.8 | async-start | bytes 1179648 | tf_op jit(solution)/shard_map/all_gather | solution.py:14
  118.0 3.5 copy-start.10
  118.0 64.3 %copy-start.5 = (f32[8,128,2]{2,1,0:T(8,128)S(1)}, f32[8,128,2]{2,1,0:T(8,128)}, u32[]{:S(2)}) copy-start(f32[8,128,2]{2,1,0:T(8,128)} %get-tuple-element.228) | copy-start | bytes 24580
  118.0 64.5 %copy-start.4 = (f32[8,128,2]{2,1,0:T(8,128)S(1)}, f32[8,128,2]{2,1,0:T(8,128)}, u32[]{:S(2)}) copy-start(f32[8,128,2]{2,1,0:T(8,128)} %get-tuple-element.235) | copy-start | bytes 24580
  118.7 111.7 %all-gather.11.cloned.1.call-start = ((), (), s32[]{:S(2)}) async-start(), calls=%async_computation.3 | async-start | bytes 10485760 | tf_op jit(solution)/shard_map/all_gather | solution.py:190
  119.5 206.9 %all-gather.13.cloned.1.call-start = ((), (), s32[]{:S(2)}) async-start(), calls=%async_computation.4 | async-start | bytes 6488064 | tf_op jit(solution)/shard_map/all_gather | solution.py:208
  120.2 298.7 %all-gather.15.cloned.1.call-start = ((), (), s32[]{:S(2)}) async-start(), calls=%async_computation.5 | async-start | bytes 6488064 | tf_op jit(solution)/shard_map/all_gather | solution.py:213
  120.8 391.4 %all-gather.17.cloned.1.call-start = ((), (), s32[]{:S(2)}) async-start(), calls=%async_computation.6 | async-start | bytes 6488064 | tf_op jit(solution)/shard_map/all_gather | solution.py:227
  121.4 456.4 %reduce-scatter.2.cloned.1.call-start = ((), (), s32[]{:S(2)}) async-start(), calls=%async_computation.7 | async-start | bytes 5242880 | tf_op jit(solution)/shard_map/reduce_scatter | solution.py:228
  182.5 12.5 %copy-start.3 = (bf16[1024,256]{1,0:T(8,128)(2,1)S(1)}, bf16[1024,256]{1,0:T(8,128)(2,1)}, u32[]{:S(2)}) copy-start(bf16[1024,256]{1,0:T(8,128)(2,1)} %param.21) | copy-start | bytes 1572868
  196.1 2.3 copy-start.9
  200.5 29.9 %copy-start.1 = (bf16[256,2048]{1,0:T(8,128)(2,1)S(1)}, bf16[256,2048]{1,0:T(8,128)(2,1)}, u32[]{:S(2)}) copy-start(bf16[256,2048]{1,0:T(8,128)(2,1)} %param.20) | copy-start | bytes 3145732
  230.5 6.0 %copy-start.8 = (f32[2048]{0:T(1024)S(1)}, f32[2048]{0:T(1024)}, u32[]{:S(2)}) copy-start(f32[2048]{0:T(1024)} %param.30) | copy-start | bytes 24580
  237.4 57.4 %copy-start.6 = (f32[3,1408]{1,0:T(4,128)S(1)}, f32[3,1408]{1,0:T(4,128)}, u32[]{:S(2)}) copy-start(f32[3,1408]{1,0:T(4,128)} %param.34) | copy-start | bytes 50692
  237.4 57.4 %copy-start.7 = (f32[3,1408]{1,0:T(4,128)S(1)}, f32[3,1408]{1,0:T(4,128)}, u32[]{:S(2)}) copy-start(f32[3,1408]{1,0:T(4,128)} %param.33) | copy-start | bytes 50692
  288.2 2.0 copy-start
  290.2 36.2 %collective-permute-start = (bf16[2,2048]{1,0:T(2,128)(2,1)S(1)}, bf16[2,2048]{1,0:T(2,128)(2,1)S(1)}, u32[]{:S(2)}, u32[]{:S(2)}) collective-permute-start(bf16[2,2048]{1,0:T(2,128)(2,1)S(1)} %slice.72), channel_id=1, source_target_pairs={{0,4},{4,8},{8,12},{12,16},{16,20},{20,24},{24,28},{1,5},{5,9},{9,... | collective-permute-start | bytes 24584 | tf_op jit(solution)/shard_map/ppermute | solution.py:35
Sparse Core Ops, SparseCore 0:
  118.8 42.9 all-gather.18
  163.4 66.7 all-gather.10
  232.5 93.8 all-gather.12
  328.4 90.4 all-gather.14
  420.8 91.3 all-gather.16
  535.0 42.7 reduce-scatter.1
